TPU v7x, 512 devices: a whole 4x8x8 slice. The times are simulated.
512 devices in a mesh: sp: 32 (over z, x), tp: 16 (over y, core).
Axes of the slice: x: 4, y: 8, z: 8, core: 2. Of those that a mesh axis runs over, the one named last changes fastest.
Arguments:
- tokens: bfloat16 [16384, 4096], P('sp', 'tp'), may hold values from -8 to 8
- w_key: bfloat16 [4096, 2048], P(None, 'tp'), may hold values from -0.09375 to 0.09375
- w_value: bfloat16 [4096, 2048], P(None, 'tp'), may hold values from -0.09375 to 0.09375
- w_beta: bfloat16 [4096, 16], replicated, may hold values from -0.09375 to 0.09375
- w_decay: bfloat16 [4096, 16], replicated, may hold values from -0.09375 to 0.09375
- beta_bias: float32 [16], replicated, may hold values from -6 to -4
- decay_rate: float32 [16], replicated, as said below
- forgetting_increment: float32 [16, 16384], P('tp', 'sp')
- new_query: bfloat16 [16, 128], P('tp', 'sp'), may hold values from -6 to 6
- read_gain: bfloat16 [128], replicated, may hold values from 0.099609375 to 1.8984375
Outputs:
- state_cache: bfloat16 [16, 128, 128], P('tp', 'sp')
- first_read: float32 [16, 128], P('tp')
Inputs may be any that keep to these rules, and one draw needn't show every extreme that they name: `decay_rate`: positive.
All inputs are finite; a program needn't handle non-finite values.
Results may differ from a plain program's by a relative error of at most 0.0075.
Values may be sent and summed in bfloat16 or wider, within the bound.
A program may use at most 64 MiB of HBM per device.

v0:
```python
import jax
import jax.numpy as jnp
from jax import lax
from jax.sharding import Mesh
from jax.sharding import PartitionSpec as P

DK = 128
DV = 128
BLOCK = 64
SP = ("sp_0", "sp_1")
norm_eps = 1e-06


def neutral_like(x, identity):
    return jnp.zeros_like(x) + jnp.asarray(identity, x.dtype)


def entering(x, axes, combine, identity):
    before = start = neutral_like(x, identity)
    running = x
    for axis in reversed(axes):
        count, mine = (lax.axis_size(axis), lax.axis_index(axis))
        pieces = lax.all_gather(running, axis)
        inside, running = (start, start)
        for k in reversed(range(count)):
            passed = k > mine
            running = combine(running, pieces[k])
            inside = jnp.where(passed, running, inside)
        before = combine(inside, before)
    return before


def cut_along(x, dim, count):
    lengths = x.shape
    pieces = x.reshape(*lengths[:dim], count, lengths[dim] // count, *lengths[dim + 1 :])
    return jnp.moveaxis(pieces, dim, 0)


def summed_on_arrival(x, axis, dim):
    pieces = cut_along(x, dim, lax.axis_size(axis))
    arrived = lax.all_to_all(pieces, axis, split_axis=0, concat_axis=0, tiled=True)
    return arrived.sum(axis=0)


def from_everyone(x, axis):
    count = lax.axis_size(axis)
    return lax.all_to_all(jnp.broadcast_to(x[None], (count, *x.shape)), axis, 0, 0, tiled=True)


def taken_together(x, axis):
    return from_everyone(x, axis).sum(axis=0)


def matmul_f32(left, right):
    return jnp.dot(left, right, precision=lax.Precision.HIGHEST)


def batched_f32(left, right):
    return jnp.einsum("hij,hjk->hik", left, right, precision=lax.Precision.HIGHEST)


def unit_inverse(lower):
    current_size = lower.shape[0]
    identity = jnp.eye(current_size, dtype=jnp.float32)
    result = identity - lower
    lower_power = lower
    covered = 2
    while covered < current_size:
        lower_power = matmul_f32(lower_power, lower_power)
        result = matmul_f32(result, identity + lower_power)
        covered = covered * 2
    return result


def block_terms(key_blk, value_blk, beta_blk, logd_blk):
    current_size = key_blk.shape[0]
    cumulative = jnp.cumsum(logd_blk)
    spread = cumulative[:, None] - cumulative[None, :]
    location_positions = jnp.arange(current_size)
    causal = location_positions[:, None] >= location_positions[None, :]
    strict = location_positions[:, None] > location_positions[None, :]
    decay_table = jnp.where(causal, jnp.exp(jnp.where(causal, spread, 0.0)), 0.0)
    key_beta = key_blk * beta_blk[:, None]
    lower = jnp.where(strict, matmul_f32(key_beta, key_blk.T) * decay_table, 0.0)
    inverse = unit_inverse(lower)
    update = matmul_f32(inverse, value_blk * beta_blk[:, None])
    erase = matmul_f32(inverse, key_beta * jnp.exp(cumulative)[:, None])
    key_remainder = key_blk * jnp.exp(cumulative[-1] - cumulative)[:, None]
    return (update, erase, key_remainder, jnp.exp(cumulative[-1]))


def per_device(
    tokens,
    w_key,
    w_value,
    w_beta,
    w_decay,
    beta_bias,
    decay_rate,
    forgetting_increment,
    new_query,
    read_gain,
):
    heads_here = w_key.shape[1] // DK
    token_count = tokens.shape[0]
    head_start = lax.axis_index("tp") * heads_here
    gate_weights = jnp.concatenate(
        [
            lax.dynamic_slice_in_dim(w_beta, head_start, heads_here, 1),
            lax.dynamic_slice_in_dim(w_decay, head_start, heads_here, 1),
        ],
        axis=1,
    )
    piece = lax.all_gather(tokens, "tp", axis=1, tiled=True)
    key_acc = jnp.dot(piece, w_key, preferred_element_type=jnp.float32)
    value_acc = jnp.dot(piece, w_value, preferred_element_type=jnp.float32)
    gate_acc = jnp.dot(piece, gate_weights, preferred_element_type=jnp.float32)
    key_wide = (
        lax.optimization_barrier(key_acc.astype(jnp.bfloat16))
        .astype(jnp.float32)
        .reshape(token_count, heads_here, DK)
    )
    key_unit = key_wide * lax.rsqrt(jnp.sum(key_wide * key_wide, axis=-1, keepdims=True) + norm_eps)
    value_wide = (
        lax.optimization_barrier(value_acc.astype(jnp.bfloat16))
        .astype(jnp.float32)
        .reshape(token_count, heads_here, DV)
    )
    bias_here = lax.dynamic_slice_in_dim(beta_bias, head_start, heads_here, 0)
    rate_here = lax.dynamic_slice_in_dim(decay_rate, head_start, heads_here, 0)
    beta = jax.nn.sigmoid(gate_acc[:, :heads_here] + bias_here).T
    log_decay = (
        -rate_here[:, None] * jax.nn.softplus(gate_acc[:, heads_here:].T) + forgetting_increment
    )
    blocks = token_count // BLOCK
    key_heads = key_unit.transpose(1, 0, 2).reshape(heads_here, blocks, BLOCK, DK)
    value_heads = value_wide.transpose(1, 0, 2).reshape(heads_here, blocks, BLOCK, DV)
    terms = jax.vmap(jax.vmap(block_terms))(
        key_heads,
        value_heads,
        beta.reshape(heads_here, blocks, BLOCK),
        log_decay.reshape(heads_here, blocks, BLOCK),
    )
    inputs = tuple((jnp.moveaxis(item, 1, 0) for item in terms))
    identity = jnp.broadcast_to(jnp.eye(DK, dtype=jnp.float32), (heads_here, DK, DK))
    value_zeros = jnp.zeros((heads_here, DK, DV), jnp.float32)
    padding = jnp.zeros((heads_here, BLOCK, DK), jnp.float32)

    def advance(state, block_in):
        update, erase, key_remainder, keep = block_in
        fresh = jnp.concatenate([update, padding], axis=-1) - jnp.einsum(
            "hcd,hde->hce", erase, state, precision=lax.Precision.HIGHEST
        )
        state = keep[:, None, None] * state + jnp.einsum(
            "hcd,hce->hde", key_remainder, fresh, precision=lax.Precision.HIGHEST
        )
        return (state, None)

    combined, _ = lax.scan(advance, jnp.concatenate([value_zeros, identity], axis=-1), inputs)
    local_b = combined[:, :, :DV]
    local_left = combined[:, :, DV:]
    later_product = entering(local_left, SP, batched_f32, identity)
    summed = summed_on_arrival(batched_f32(later_product, local_b), SP, 1)
    own_rows = summed.astype(jnp.bfloat16)
    partial_read = jnp.sum(
        new_query.astype(jnp.float32)[:, :, None] * own_rows.astype(jnp.float32), axis=1
    )
    raw_read = taken_together(partial_read, SP)
    first_read = (
        raw_read
        * lax.rsqrt(jnp.mean(raw_read * raw_read, axis=-1, keepdims=True) + norm_eps)
        * read_gain.astype(jnp.float32)
    )
    return (own_rows, first_read)


def solution(mesh):
    finer = Mesh(mesh.devices.reshape(8, 4, mesh.shape["tp"]), ("sp_0", "sp_1", "tp"))
    return jax.shard_map(
        per_device,
        mesh=finer,
        in_specs=(
            P(SP, "tp"),
            P(None, "tp"),
            P(None, "tp"),
            P(),
            P(),
            P(),
            P(),
            P("tp", SP),
            P("tp", SP),
            P(),
        ),
        out_specs=(P("tp", SP, None), P("tp", None)),
        check_vma=False,
    )
```

profile of v0, /device:TPU:8, one launch (start us, length us, event | category | flops | bytes accessed | tf_op | source)
XLA Modules:
  0.0 179.6 jit_solution(8949332273028373998)
XLA Ops:
  7.2 0.7 all-gather.4.cloned.1.call-update
  8.0 1.2 dynamic_slice.26
  9.8 1.3 dynamic_slice.29
  11.2 0.9 constant_dynamic-slice_fusion.1
  12.1 53.6 %all-gather.4.cloned.1.call-done = bf16[512,4096]{1,0:T(8,128)(2,1)} async-done(((bf16[512,256]{1,0:T(8,128)(2,1)}), bf16[512,4096]{1,0:T(8,128)(2,1)}) %all-gather.4.cloned.1.call-update) | async-done | bytes 4194320 | tf_op jit(solution)/shard_map/all_gather | solution.py:114
  65.7 3.5 %convolution_bitcast_fusion.5 = f32[512,2]{0,1:T(2,128)S(1)} fusion(bf16[512,4096]{1,0:T(8,128)(2,1)} %all-gather.4.cloned.1.call-done, bf16[4096,1]{0,1:T(2,128)(2,1)S(1)} %get-tuple-element.81, bf16[4096,1]{0,1:T(2,128)(2,1)S(1)} %get-tuple-element.82), kind=kOutput, calls=%fused_computation.23 | convolution fusion | flops 8421376 | bytes 4214784 | tf_op jit(solution)/shard_map/dot_general | solution.py:117
  69.1 0.7 fusion.77
  70.5 3.6 %convolution_convert_fusion.1 = bf16[512,128]{1,0:T(8,128)(2,1)S(1)} fusion(bf16[512,4096]{1,0:T(8,128)(2,1)} %all-gather.4.cloned.1.call-done, bf16[4096,128]{1,0:T(8,128)(2,1)S(1)} %copy-done), kind=kOutput, calls=%fused_computation.20 | convolution fusion | flops 536936448 | bytes 5373952 | tf_op jit(solution)/shard_map/dot_general | solution.py:115
  74.1 1.3 convolution_convert_fusion
  81.4 14.6 %while.10 = (s32[]{:T(128)}, f32[1,128,256]{2,1,0:T(8,128)S(1)}, f32[8,1]{0,1:T(1,128)S(1)}, f32[8,1,64,128]{3,2,1,0:T(8,128)S(1)}, f32[8,1,64,128]{3,2,1,0:T(8,...) while((s32[]{:T(128)}, f32[1,128,256]{2,1,0:T(8,128)S(1)}, f32[8,1]{0,1:T(1,128)S(1)}, ...), condition=%wide.region_3.4_spmd, body=%wide.region_2.3_spmd.sunk | while | flops 50413568 | bytes 688241 | solution.py:159
  82.2 1.0 fusion.133
  84.0 1.0 fusion.133
  85.9 1.0 fusion.133
  87.7 1.0 fusion.133
  89.5 1.0 fusion.133
  91.4 1.0 fusion.133
  93.2 1.0 fusion.133
  95.0 1.0 fusion.133
  96.1 12.6 %all-gather = f32[4,128,128]{2,1,0:T(8,128)S(1)} all-gather(f32[1,128,128]{2,1,0:T(8,128)S(1)} %slice.55), channel_id=2, replica_groups=mesh['sp_0'=8,'sp_1'=4,'tp'=16] {'sp_1'}, dimensions={0}, use_global_device_ids=true | all-gather | bytes 327680 | tf_op jit(solution)/shard_map/all_gather | solution.py:23
  109.5 27.6 %all-gather.1 = f32[1024,128]{1,0:T(8,128)S(1)} all-gather(f32[128,128]{1,0:T(8,128)S(1)} %fusion.56), channel_id=3, replica_groups=mesh['sp_0'=8,'sp_1'=4,'tp'=16] {'sp_0'}, dimensions={0}, use_global_device_ids=true | all-gather | bytes 589824 | tf_op jit(solution)/shard_map/all_gather | solution.py:23
  139.3 0.7 copy.34
  140.0 7.9 %all-to-all-start = ((f32[32,1,4,128]{3,2,1,0:T(4,128)}), f32[32,1,4,128]{3,2,1,0:T(4,128)S(1)}, u32[]{:S(2)}, u32[]{:S(2)}) async-start(f32[32,1,4,128]{3,2,1,0:T(4,128)} %copy.34), calls=%async_computation | async-start | bytes 131072 | tf_op jit(solution)/shard_map/all_to_all | solution.py:41
  147.9 9.9 %all-to-all-done = f32[32,1,4,128]{3,2,1,0:T(4,128)S(1)} async-done(((f32[32,1,4,128]{3,2,1,0:T(4,128)}), f32[32,1,4,128]{3,2,1,0:T(4,128)S(1)}, u32[]{:S(2)}, u32[]{:S(2)}) %all-to-all-start) | async-done | bytes 65568 | tf_op jit(solution)/shard_map/all_to_all | solution.py:41
  158.0 12.9 %all_to_all.10 = f32[32,1,128]{2,1,0:T(1,128)S(1)} all-to-all(f32[32,1,128]{2,1,0:T(1,128)S(1)} %broadcast_in_dim.21), channel_id=1, replica_groups=mesh['sp_0'=8,'sp_1'=4,'tp'=16] {'sp_0','sp_1'}, dimensions={0} | all-to-all | bytes 32768 | tf_op jit(solution)/shard_map/all_to_all | solution.py:47
  (89 shorter events, 17.3 us)
Async XLA Ops:
  7.2 63.3 %copy-start = (bf16[4096,128]{1,0:T(8,128)(2,1)S(1)}, bf16[4096,128]{1,0:T(8,128)(2,1)}, u32[]{:S(2)}) copy-start(bf16[4096,128]{1,0:T(8,128)(2,1)} %param.13) | copy-start | bytes 3145732
  7.2 62.7 %copy-start.3 = (f32[1,512]{1,0:T(1,128)S(1)}, f32[1,512]{1,0:T(1,128)}, u32[]{:S(2)}) copy-start(f32[1,512]{1,0:T(1,128)} %param.19) | copy-start | bytes 6148
  7.2 58.5 %all-gather.4.cloned.1.call-start = ((), (), s32[]{:S(2)}) async-start(), calls=%async_computation.2 | async-start | bytes 4456448 | tf_op jit(solution)/shard_map/all_gather | solution.py:114
  65.7 8.4 %copy-start.5 = (bf16[4096,128]{1,0:T(8,128)(2,1)S(1)}, bf16[4096,128]{1,0:T(8,128)(2,1)}, u32[]{:S(2)}) copy-start(bf16[4096,128]{1,0:T(8,128)(2,1)} %param.14) | copy-start | bytes 3145732
  70.2 3.9 %copy-start.1 = (bf16[512,4096]{1,0:T(8,128)(2,1)S(1)}, bf16[512,4096]{1,0:T(8,128)(2,1)}, u32[]{:S(2)}) copy-start(bf16[512,4096]{1,0:T(8,128)(2,1)} %all-gather.4.cloned.1.call-done) | copy-start | bytes 12582916
  81.4 66.5 %copy-start.6 = (bf16[1,4]{1,0:T(2,128)(2,1)S(1)}, bf16[1,4]{1,0:T(2,128)(2,1)}, u32[]{:S(2)}) copy-start(bf16[1,4]{1,0:T(2,128)(2,1)} %param.20) | copy-start | bytes 28
  81.4 90.8 %copy-start.4 = (bf16[128]{0:T(256)(128)(2,1)S(1)}, bf16[128]{0:T(256)(128)(2,1)}, u32[]{:S(2)}) copy-start(bf16[128]{0:T(256)(128)(2,1)} %param.21) | copy-start | bytes 772
  140.0 17.9 %all-to-all-start = ((f32[32,1,4,128]{3,2,1,0:T(4,128)}), f32[32,1,4,128]{3,2,1,0:T(4,128)S(1)}, u32[]{:S(2)}, u32[]{:S(2)}) async-start(f32[32,1,4,128]{3,2,1,0:T(4,128)} %copy.34), calls=%async_computation | async-start | bytes 131072 | tf_op jit(solution)/shard_map/all_to_all | solution.py:41
  157.9 14.8 %copy-start.2 = (bf16[4,128]{1,0:T(4,128)(2,1)}, bf16[4,128]{1,0:T(4,128)(2,1)S(1)}, u32[]{:S(2)}) copy-start(bf16[4,128]{1,0:T(4,128)(2,1)S(1)} %reduce_sum.46) | copy-start | bytes 3076
Sparse Core Ops, SparseCore 0:
  10.0 55.5 all-gather.3
where the time goes:
time: 180 us
  waiting for transfers between devices  64.2 us (36%)
  blocking collectives  53 us (29%)
  matrix products  26.5 us (15%)
  between operations  15.8 us (9%)
  local copies, waits for them, and re-layouts  9.17 us (5%)
  starting transfers between devices  7.96 us (4%)
  other arithmetic  2.73 us (2%)
    all_gather x1, waiting for transfers between devices, per_device(): piece = lax.all_gather(tokens, 'tp', axis=1, tiled=True)  53.6 us
    all_gather x2, blocking collectives, entering(): pieces = lax.all_gather(running, axis)  40.2 us
    all_to_all x1, blocking collectives, from_everyone(): lax.all_to_all(jnp.broadcast_to(x[None], (count, *x.shape)), axis, 0, 0,...  12.9 us
    all_to_all x1, waiting for transfers between devices, summed_on_arrival(): lax.all_to_all(pieces, axis, split_axis=0, concat_axis=0, tiled=True)  9.95 us
    dot_general x8, matrix products, advance(): jnp.einsum('hcd,hce->hde', key_remainder, fresh, precision=lax.Precision....  8.06 us
    all_to_all x1, starting transfers between devices, summed_on_arrival(): lax.all_to_all(pieces, axis, split_axis=0, concat_axis=0, tiled=True)  7.92 us
    dot_general x13, matrix products, matmul_f32(): return jnp.dot(left, right, precision=lax.Precision.HIGHEST)  5.5 us
    dynamic_slice x8, local copies, waits for them, and re-layouts, per_device(): lax.scan(advance, jnp.concatenate([value_zeros, identity], axis=-1), inputs)  4.68 us
  transfers between devices with their start and end apart: 2, of which 2 were waited for; matrix products, arithmetic and copies ran while one was open for 2% of the time, Pallas kernels for 0%

commit v1 on v0

--- a/solution.py
+++ b/solution.py
@@ -1,3 +1,4 @@
+import functools
 import jax
 import jax.numpy as jnp
 from jax import lax
@@ -9,6 +10,35 @@
 BLOCK = 64
 SP = ("sp_0", "sp_1")
 norm_eps = 1e-06
+
+
+def _extend_object(arr, in_dim):
+    arr = jnp.moveaxis(arr, 0, in_dim)
+    front = arr.shape
+    return arr.reshape(*front[:in_dim], front[in_dim] * front[in_dim + 1], *front[in_dim + 2 :])
+
+
+def inputs_name(here_x, mesh_name, row_dim):
+    sides = lax.psum(1, mesh_name)
+    w1 = map(lambda c: (c, (c + 1) % sides), range(sides))
+    pages = list(w1)
+    buffers = [(b, w) for w, b in pages]
+    outcome_arr, frame_out = ([], [])
+    for ii in range(sides - 1):
+        if ii % 2 == 0:
+            y_new = lax.ppermute(outcome_arr[-1] if outcome_arr else here_x, mesh_name, pages)
+            outcome_arr.append(y_new)
+        else:
+            current_block = lax.ppermute(frame_out[-1] if frame_out else here_x, mesh_name, buffers)
+            frame_out.append(current_block)
+    v1 = jnp.stack([*outcome_arr[::-1], here_x, *frame_out], 0)
+    top = lax.axis_index(mesh_name)
+    local_part = top - len(outcome_arr)
+    v1 = v1[(jnp.arange(sides) - local_part) % sides]
+    return _extend_object(v1, row_dim)
+
+
+define_patch_on = functools.partial(inputs_name, mesh_name="tp", row_dim=1)
 
 
 def neutral_like(x, identity):
@@ -111,7 +141,7 @@
         ],
         axis=1,
     )
-    piece = lax.all_gather(tokens, "tp", axis=1, tiled=True)
+    piece = define_patch_on(tokens)
     key_acc = jnp.dot(piece, w_key, preferred_element_type=jnp.float32)
     value_acc = jnp.dot(piece, w_value, preferred_element_type=jnp.float32)
     gate_acc = jnp.dot(piece, gate_weights, preferred_element_type=jnp.float32)

time: 180 us -> 195 us (1.083)
  the two profiles are of different devices: /device:TPU:8 before, /device:TPU:32 now
where the time goes in v1:
time: 195 us
  blocking collectives  57.6 us (30%)
  waiting for transfers between devices  40.8 us (21%)
  local copies, waits for them, and re-layouts  38.5 us (20%)
  starting transfers between devices  27.4 us (14%)
  matrix products  25 us (13%)
  other arithmetic  2.67 us (1%)
  between operations  2.46 us (1%)
    all_gather x2, blocking collectives, entering(): pieces = lax.all_gather(running, axis)  44.8 us
    ppermute x8, waiting for transfers between devices, inputs_name(): lax.ppermute(outcome_arr[-1] if outcome_arr else here_x, mesh_name, pages)  29.4 us
    ppermute x7, starting transfers between devices, inputs_name(): lax.ppermute(frame_out[-1] if frame_out else here_x, mesh_name, buffers)  21.3 us
    unnamed x37, local copies, waits for them, and re-layouts  17.2 us
    all_to_all x1, blocking collectives, from_everyone(): lax.all_to_all(jnp.broadcast_to(x[None], (count, *x.shape)), axis, 0, 0,...  12.9 us
    all_to_all x1, waiting for transfers between devices, summed_on_arrival(): lax.all_to_all(pieces, axis, split_axis=0, concat_axis=0, tiled=True)  9.95 us
    dot_general x8, matrix products, advance(): jnp.einsum('hcd,hce->hde', key_remainder, fresh, precision=lax.Precision....  8.04 us
    transpose x1, local copies, waits for them, and re-layouts, _extend_object(): arr = jnp.moveaxis(arr, 0, in_dim)  6.41 us
  transfers between devices with their start and end apart: 16, of which 11 were waited for; matrix products, arithmetic and copies ran while one was open for 10% of the time, Pallas kernels for 0%

profile of v1, /device:TPU:32, one launch (start us, length us, event | category | flops | bytes accessed | tf_op | source)
XLA Modules:
  0.0 194.7 jit_solution(6173698594218950476)
XLA Ops:
  0.7 7.2 %collective-permute-done = bf16[512,256]{1,0:T(8,128)(2,1)S(1)} collective-permute-done((bf16[512,256]{1,0:T(8,128)(2,1)}, bf16[512,256]{1,0:T(8,128)(2,1)S(1)}, u32[]{:S(2)}, u32[]{:S(2)}) %collective-permute-start) | collective-permute-done | bytes 262176 | tf_op jit(solution)/shard_map/ppermute | solution.py:29
  7.9 3.0 %collective-permute-start.8 = (bf16[512,256]{1,0:T(8,128)(2,1)}, bf16[512,256]{1,0:T(8,128)(2,1)S(1)}, u32[]{:S(2)}, u32[]{:S(2)}) collective-permute-start(bf16[512,256]{1,0:T(8,128)(2,1)} %param.12), channel_id=1, source_target_pairs={{1,0},{2,1},{3,2},{4,3},{5,4},{6,5},{7,6},{8,7},{9,8},{10,9},{11,1... | collective-permute-start | bytes 786440 | tf_op jit(solution)/shard_map/ppermute | solution.py:32
  10.9 4.1 %collective-permute-done.1 = bf16[512,256]{1,0:T(8,128)(2,1)S(1)} collective-permute-done((bf16[512,256]{1,0:T(8,128)(2,1)S(1)}, bf16[512,256]{1,0:T(8,128)(2,1)S(1)}, u32[]{:S(2)}, u32[]{:S(2)}) %collective-permute-start.1) | collective-permute-done | bytes 262176 | tf_op jit(solution)/shard_map/ppermute | solution.py:29
  15.1 3.0 %collective-permute-start.9 = (bf16[512,256]{1,0:T(8,128)(2,1)S(1)}, bf16[512,256]{1,0:T(8,128)(2,1)S(1)}, u32[]{:S(2)}, u32[]{:S(2)}) collective-permute-start(bf16[512,256]{1,0:T(8,128)(2,1)S(1)} %collective-permute-done.8), channel_id=1, source_target_pairs={{1,0},{2,1},{3,2},{4,3},{5,4},{6,5},{7,6},{8,7},{9,8},{10,9},{11,1... | collective-permute-start | bytes 786440 | tf_op jit(solution)/shard_map/ppermute | solution.py:32
  18.1 3.8 %collective-permute-done.2 = bf16[512,256]{1,0:T(8,128)(2,1)S(1)} collective-permute-done((bf16[512,256]{1,0:T(8,128)(2,1)S(1)}, bf16[512,256]{1,0:T(8,128)(2,1)S(1)}, u32[]{:S(2)}, u32[]{:S(2)}) %collective-permute-start.2) | collective-permute-done | bytes 262176 | tf_op jit(solution)/shard_map/ppermute | solution.py:29
  22.0 3.1 %collective-permute-start.10 = (bf16[512,256]{1,0:T(8,128)(2,1)S(1)}, bf16[512,256]{1,0:T(8,128)(2,1)S(1)}, u32[]{:S(2)}, u32[]{:S(2)}) collective-permute-start(bf16[512,256]{1,0:T(8,128)(2,1)S(1)} %collective-permute-done.9), channel_id=1, source_target_pairs={{1,0},{2,1},{3,2},{4,3},{5,4},{6,5},{7,6},{8,7},{9,8},{10,9},{11,1... | collective-permute-start | bytes 786440 | tf_op jit(solution)/shard_map/ppermute | solution.py:32
  25.1 3.8 %collective-permute-done.3 = bf16[512,256]{1,0:T(8,128)(2,1)S(1)} collective-permute-done((bf16[512,256]{1,0:T(8,128)(2,1)S(1)}, bf16[512,256]{1,0:T(8,128)(2,1)S(1)}, u32[]{:S(2)}, u32[]{:S(2)}) %collective-permute-start.3) | collective-permute-done | bytes 262176 | tf_op jit(solution)/shard_map/ppermute | solution.py:29
  29.0 3.1 %collective-permute-start.11 = (bf16[512,256]{1,0:T(8,128)(2,1)S(1)}, bf16[512,256]{1,0:T(8,128)(2,1)S(1)}, u32[]{:S(2)}, u32[]{:S(2)}) collective-permute-start(bf16[512,256]{1,0:T(8,128)(2,1)S(1)} %collective-permute-done.10), channel_id=1, source_target_pairs={{1,0},{2,1},{3,2},{4,3},{5,4},{6,5},{7,6},{8,7},{9,8},{10,9},{11,1... | collective-permute-start | bytes 786440 | tf_op jit(solution)/shard_map/ppermute | solution.py:32
  32.1 3.9 %collective-permute-done.4 = bf16[512,256]{1,0:T(8,128)(2,1)} collective-permute-done((bf16[512,256]{1,0:T(8,128)(2,1)S(1)}, bf16[512,256]{1,0:T(8,128)(2,1)}, u32[]{:S(2)}, u32[]{:S(2)}) %collective-permute-start.4) | collective-permute-done | bytes 262176 | tf_op jit(solution)/shard_map/ppermute | solution.py:29
  37.7 3.0 %collective-permute-start.12 = (bf16[512,256]{1,0:T(8,128)(2,1)S(1)}, bf16[512,256]{1,0:T(8,128)(2,1)}, u32[]{:S(2)}, u32[]{:S(2)}) collective-permute-start(bf16[512,256]{1,0:T(8,128)(2,1)S(1)} %collective-permute-done.11), channel_id=1, source_target_pairs={{1,0},{2,1},{3,2},{4,3},{5,4},{6,5},{7,6},{8,7},{9,8},{10,9},{11,1... | collective-permute-start | bytes 786440 | tf_op jit(solution)/shard_map/ppermute | solution.py:32
  40.7 2.6 %collective-permute-done.5 = bf16[512,256]{1,0:T(8,128)(2,1)S(1)} collective-permute-done((bf16[512,256]{1,0:T(8,128)(2,1)}, bf16[512,256]{1,0:T(8,128)(2,1)S(1)}, u32[]{:S(2)}, u32[]{:S(2)}) %collective-permute-start.5) | collective-permute-done | bytes 262176 | tf_op jit(solution)/shard_map/ppermute | solution.py:29
  44.5 3.2 %collective-permute-start.13 = (bf16[512,256]{1,0:T(8,128)(2,1)}, bf16[512,256]{1,0:T(8,128)(2,1)}, u32[]{:S(2)}, u32[]{:S(2)}) collective-permute-start(bf16[512,256]{1,0:T(8,128)(2,1)} %collective-permute-done.12), channel_id=1, source_target_pairs={{1,0},{2,1},{3,2},{4,3},{5,4},{6,5},{7,6},{8,7},{9,8},{10,9},{11,1... | collective-permute-start | bytes 786440 | tf_op jit(solution)/shard_map/ppermute | solution.py:32
  47.8 2.6 %collective-permute-done.6 = bf16[512,256]{1,0:T(8,128)(2,1)} collective-permute-done((bf16[512,256]{1,0:T(8,128)(2,1)S(1)}, bf16[512,256]{1,0:T(8,128)(2,1)}, u32[]{:S(2)}, u32[]{:S(2)}) %collective-permute-start.6) | collective-permute-done | bytes 262176 | tf_op jit(solution)/shard_map/ppermute | solution.py:29
  53.6 2.9 %collective-permute-start.14 = (bf16[512,256]{1,0:T(8,128)(2,1)}, bf16[512,256]{1,0:T(8,128)(2,1)S(1)}, u32[]{:S(2)}, u32[]{:S(2)}) collective-permute-start(bf16[512,256]{1,0:T(8,128)(2,1)} %collective-permute-done.13), channel_id=1, source_target_pairs={{1,0},{2,1},{3,2},{4,3},{5,4},{6,5},{7,6},{8,7},{9,8},{10,9},{11,1... | collective-permute-start | bytes 786440 | tf_op jit(solution)/shard_map/ppermute | solution.py:32
  74.9 5.0 %gather_fusion = bf16[16,512,256]{2,1,0:T(8,128)(2,1)} fusion(bf16[16,512,256]{2,1,0:T(8,128)(2,1)} %bitcast_dynamic-update-slice_fusion, s32[1024]{0:T(1024)S(1)} %pad_clamp_fusion), kind=kCustom, calls=%fused_computation | custom fusion | bytes 8388672 | tf_op jit(solution)/shard_map/gather | solution.py:37
  79.9 6.4 %copy.37 = bf16[512,16,256]{0,2,1:T(8,128)(2,1)} copy(bf16[512,16,256]{2,0,1:T(8,128)(2,1)} %bitcast.172) | data formatting | bytes 8388608 | tf_op jit(solution)/shard_map/transpose | solution.py:16
  86.3 3.6 %convolution_convert_fusion.1 = bf16[512,128]{1,0:T(8,128)(2,1)S(1)} fusion(bf16[512,4096]{0,1:T(8,128)(2,1)} %bitcast.169, bf16[4096,128]{1,0:T(8,128)(2,1)S(1)} %copy-done), kind=kOutput, calls=%fused_computation.21 | convolution fusion | flops 536936448 | bytes 5373952 | tf_op jit(solution)/shard_map/dot_general | solution.py:145
  96.3 2.5 %convolution_convert_fusion = bf16[512,128]{1,0:T(8,128)(2,1)S(1)} fusion(bf16[512,4096]{0,1:T(8,128)(2,1)S(1)} %bitcast.171, bf16[4096,128]{1,0:T(8,128)(2,1)} %param.14), kind=kOutput, calls=%fused_computation.20 | convolution fusion | flops 536936448 | bytes 5373952 | tf_op jit(solution)/shard_map/dot_general | solution.py:146
  100.5 14.8 %while.10 = (s32[]{:T(128)}, f32[1,128,256]{2,1,0:T(8,128)S(1)}, f32[8,1]{0,1:T(1,128)S(1)}, f32[8,1,64,128]{3,2,1,0:T(8,128)S(1)}, f32[8,1,64,128]{3,2,1,0:T(8,...) while((s32[]{:T(128)}, f32[1,128,256]{2,1,0:T(8,128)S(1)}, f32[8,1]{0,1:T(1,128)S(1)}, ...), condition=%wide.region_3.4_spmd, body=%wide.region_2.3_spmd.sunk | while | flops 50413568 | bytes 688233 | solution.py:189
  115.3 12.7 %all-gather = f32[4,128,128]{2,1,0:T(8,128)S(1)} all-gather(f32[1,128,128]{2,1,0:T(8,128)S(1)} %slice.55), channel_id=2, replica_groups=mesh['sp_0'=8,'sp_1'=4,'tp'=16] {'sp_1'}, dimensions={0}, use_global_device_ids=true | all-gather | bytes 327680 | tf_op jit(solution)/shard_map/all_gather | solution.py:53
  128.8 32.0 %all-gather.1 = f32[1024,128]{1,0:T(8,128)S(1)} all-gather(f32[128,128]{1,0:T(8,128)S(1)} %fusion.56), channel_id=3, replica_groups=mesh['sp_0'=8,'sp_1'=4,'tp'=16] {'sp_0'}, dimensions={0}, use_global_device_ids=true | all-gather | bytes 589824 | tf_op jit(solution)/shard_map/all_gather | solution.py:53
  163.8 6.0 %all-to-all-start = ((f32[32,1,4,128]{3,2,1,0:T(4,128)}), f32[32,1,4,128]{3,2,1,0:T(4,128)S(1)}, u32[]{:S(2)}, u32[]{:S(2)}) async-start(f32[32,1,4,128]{3,2,1,0:T(4,128)} %copy.42), calls=%async_computation | async-start | bytes 131072 | tf_op jit(solution)/shard_map/all_to_all | solution.py:71
  169.9 9.9 %all-to-all-done = f32[32,1,4,128]{3,2,1,0:T(4,128)S(1)} async-done(((f32[32,1,4,128]{3,2,1,0:T(4,128)}), f32[32,1,4,128]{3,2,1,0:T(4,128)S(1)}, u32[]{:S(2)}, u32[]{:S(2)}) %all-to-all-start) | async-done | bytes 65568 | tf_op jit(solution)/shard_map/all_to_all | solution.py:71
  179.9 12.9 %all_to_all.10 = f32[32,1,128]{2,1,0:T(1,128)S(1)} all-to-all(f32[32,1,128]{2,1,0:T(1,128)S(1)} %broadcast_in_dim.21), channel_id=1, replica_groups=mesh['sp_0'=8,'sp_1'=4,'tp'=16] {'sp_0','sp_1'}, dimensions={0} | all-to-all | bytes 32768 | tf_op jit(solution)/shard_map/all_to_all | solution.py:77
  (144 shorter events, 51.3 us)
Async XLA Ops:
  0.6 85.7 %copy-start = (bf16[4096,128]{1,0:T(8,128)(2,1)S(1)}, bf16[4096,128]{1,0:T(8,128)(2,1)}, u32[]{:S(2)}) copy-start(bf16[4096,128]{1,0:T(8,128)(2,1)} %param.13) | copy-start | bytes 3145732
  0.6 66.6 %copy-start.3 = (bf16[512,256]{1,0:T(8,128)(2,1)S(1)}, bf16[512,256]{1,0:T(8,128)(2,1)}, u32[]{:S(2)}) copy-start(bf16[512,256]{1,0:T(8,128)(2,1)} %param.12) | copy-start | bytes 786436
  0.7 7.3 %collective-permute-start = (bf16[512,256]{1,0:T(8,128)(2,1)}, bf16[512,256]{1,0:T(8,128)(2,1)S(1)}, u32[]{:S(2)}, u32[]{:S(2)}) collective-permute-start(bf16[512,256]{1,0:T(8,128)(2,1)} %param.12), channel_id=1, source_target_pairs={{0,1},{1,2},{2,3},{3,4},{4,5},{5,6},{6,7},{7,8},{8,9},{9,10},{10,1... | collective-permute-start | bytes 786440 | tf_op jit(solution)/shard_map/ppermute | solution.py:29
  7.9 7.0 %collective-permute-start.1 = (bf16[512,256]{1,0:T(8,128)(2,1)S(1)}, bf16[512,256]{1,0:T(8,128)(2,1)S(1)}, u32[]{:S(2)}, u32[]{:S(2)}) collective-permute-start(bf16[512,256]{1,0:T(8,128)(2,1)S(1)} %collective-permute-done), channel_id=1, source_target_pairs={{0,1},{1,2},{2,3},{3,4},{4,5},{5,6},{6,7},{7,8},{8,9},{9,10},{10,1... | collective-permute-start | bytes 786440 | tf_op jit(solution)/shard_map/ppermute | solution.py:29
  7.9 7.2 %collective-permute-start.8 = (bf16[512,256]{1,0:T(8,128)(2,1)}, bf16[512,256]{1,0:T(8,128)(2,1)S(1)}, u32[]{:S(2)}, u32[]{:S(2)}) collective-permute-start(bf16[512,256]{1,0:T(8,128)(2,1)} %param.12), channel_id=1, source_target_pairs={{1,0},{2,1},{3,2},{4,3},{5,4},{6,5},{7,6},{8,7},{9,8},{10,9},{11,1... | collective-permute-start | bytes 786440 | tf_op jit(solution)/shard_map/ppermute | solution.py:32
  14.9 7.0 %collective-permute-start.2 = (bf16[512,256]{1,0:T(8,128)(2,1)S(1)}, bf16[512,256]{1,0:T(8,128)(2,1)S(1)}, u32[]{:S(2)}, u32[]{:S(2)}) collective-permute-start(bf16[512,256]{1,0:T(8,128)(2,1)S(1)} %collective-permute-done.1), channel_id=1, source_target_pairs={{0,1},{1,2},{2,3},{3,4},{4,5},{5,6},{6,7},{7,8},{8,9},{9,10},{10,1... | collective-permute-start | bytes 786440 | tf_op jit(solution)/shard_map/ppermute | solution.py:29
  15.1 6.9 %collective-permute-start.9 = (bf16[512,256]{1,0:T(8,128)(2,1)S(1)}, bf16[512,256]{1,0:T(8,128)(2,1)S(1)}, u32[]{:S(2)}, u32[]{:S(2)}) collective-permute-start(bf16[512,256]{1,0:T(8,128)(2,1)S(1)} %collective-permute-done.8), channel_id=1, source_target_pairs={{1,0},{2,1},{3,2},{4,3},{5,4},{6,5},{7,6},{8,7},{9,8},{10,9},{11,1... | collective-permute-start | bytes 786440 | tf_op jit(solution)/shard_map/ppermute | solution.py:32
  21.9 7.0 %collective-permute-start.3 = (bf16[512,256]{1,0:T(8,128)(2,1)S(1)}, bf16[512,256]{1,0:T(8,128)(2,1)S(1)}, u32[]{:S(2)}, u32[]{:S(2)}) collective-permute-start(bf16[512,256]{1,0:T(8,128)(2,1)S(1)} %collective-permute-done.2), channel_id=1, source_target_pairs={{0,1},{1,2},{2,3},{3,4},{4,5},{5,6},{6,7},{7,8},{8,9},{9,10},{10,1... | collective-permute-start | bytes 786440 | tf_op jit(solution)/shard_map/ppermute | solution.py:29
  22.0 7.0 %collective-permute-start.10 = (bf16[512,256]{1,0:T(8,128)(2,1)S(1)}, bf16[512,256]{1,0:T(8,128)(2,1)S(1)}, u32[]{:S(2)}, u32[]{:S(2)}) collective-permute-start(bf16[512,256]{1,0:T(8,128)(2,1)S(1)} %collective-permute-done.9), channel_id=1, source_target_pairs={{1,0},{2,1},{3,2},{4,3},{5,4},{6,5},{7,6},{8,7},{9,8},{10,9},{11,1... | collective-permute-start | bytes 786440 | tf_op jit(solution)/shard_map/ppermute | solution.py:32
  29.0 7.1 %collective-permute-start.4 = (bf16[512,256]{1,0:T(8,128)(2,1)S(1)}, bf16[512,256]{1,0:T(8,128)(2,1)}, u32[]{:S(2)}, u32[]{:S(2)}) collective-permute-start(bf16[512,256]{1,0:T(8,128)(2,1)S(1)} %collective-permute-done.3), channel_id=1, source_target_pairs={{0,1},{1,2},{2,3},{3,4},{4,5},{5,6},{6,7},{7,8},{8,9},{9,10},{10,1... | collective-permute-start | bytes 786440 | tf_op jit(solution)/shard_map/ppermute | solution.py:29
  29.0 8.0 %collective-permute-start.11 = (bf16[512,256]{1,0:T(8,128)(2,1)S(1)}, bf16[512,256]{1,0:T(8,128)(2,1)S(1)}, u32[]{:S(2)}, u32[]{:S(2)}) collective-permute-start(bf16[512,256]{1,0:T(8,128)(2,1)S(1)} %collective-permute-done.10), channel_id=1, source_target_pairs={{1,0},{2,1},{3,2},{4,3},{5,4},{6,5},{7,6},{8,7},{9,8},{10,9},{11,1... | collective-permute-start | bytes 786440 | tf_op jit(solution)/shard_map/ppermute | solution.py:32
  36.1 7.2 %collective-permute-start.5 = (bf16[512,256]{1,0:T(8,128)(2,1)}, bf16[512,256]{1,0:T(8,128)(2,1)S(1)}, u32[]{:S(2)}, u32[]{:S(2)}) collective-permute-start(bf16[512,256]{1,0:T(8,128)(2,1)} %collective-permute-done.4), channel_id=1, source_target_pairs={{0,1},{1,2},{2,3},{3,4},{4,5},{5,6},{6,7},{7,8},{8,9},{9,10},{10,1... | collective-permute-start | bytes 786440 | tf_op jit(solution)/shard_map/ppermute | solution.py:29
  37.7 6.8 %collective-permute-start.12 = (bf16[512,256]{1,0:T(8,128)(2,1)S(1)}, bf16[512,256]{1,0:T(8,128)(2,1)}, u32[]{:S(2)}, u32[]{:S(2)}) collective-permute-start(bf16[512,256]{1,0:T(8,128)(2,1)S(1)} %collective-permute-done.11), channel_id=1, source_target_pairs={{1,0},{2,1},{3,2},{4,3},{5,4},{6,5},{7,6},{8,7},{9,8},{10,9},{11,1... | collective-permute-start | bytes 786440 | tf_op jit(solution)/shard_map/ppermute | solution.py:32
  43.3 7.1 %collective-permute-start.6 = (bf16[512,256]{1,0:T(8,128)(2,1)S(1)}, bf16[512,256]{1,0:T(8,128)(2,1)}, u32[]{:S(2)}, u32[]{:S(2)}) collective-permute-start(bf16[512,256]{1,0:T(8,128)(2,1)S(1)} %collective-permute-done.5), channel_id=1, source_target_pairs={{0,1},{1,2},{2,3},{3,4},{4,5},{5,6},{6,7},{7,8},{8,9},{9,10},{10,1... | collective-permute-start | bytes 786440 | tf_op jit(solution)/shard_map/ppermute | solution.py:29
  44.5 9.0 %collective-permute-start.13 = (bf16[512,256]{1,0:T(8,128)(2,1)}, bf16[512,256]{1,0:T(8,128)(2,1)}, u32[]{:S(2)}, u32[]{:S(2)}) collective-permute-start(bf16[512,256]{1,0:T(8,128)(2,1)} %collective-permute-done.12), channel_id=1, source_target_pairs={{1,0},{2,1},{3,2},{4,3},{5,4},{6,5},{7,6},{8,7},{9,8},{10,9},{11,1... | collective-permute-start | bytes 786440 | tf_op jit(solution)/shard_map/ppermute | solution.py:32
  50.4 7.3 %collective-permute-start.7 = (bf16[512,256]{1,0:T(8,128)(2,1)}, bf16[512,256]{1,0:T(8,128)(2,1)}, u32[]{:S(2)}, u32[]{:S(2)}) collective-permute-start(bf16[512,256]{1,0:T(8,128)(2,1)} %collective-permute-done.6), channel_id=1, source_target_pairs={{0,1},{1,2},{2,3},{3,4},{4,5},{5,6},{6,7},{7,8},{8,9},{9,10},{10,1... | collective-permute-start | bytes 786440 | tf_op jit(solution)/shard_map/ppermute | solution.py:29
  53.5 16.6 %copy-start.5 = (bf16[512,256]{1,0:T(8,128)(2,1)S(1)}, bf16[512,256]{1,0:T(8,128)(2,1)}, u32[]{:S(2)}) copy-start(bf16[512,256]{1,0:T(8,128)(2,1)} %copy-done.4) | copy-start | bytes 786436
  53.6 20.6 %collective-permute-start.14 = (bf16[512,256]{1,0:T(8,128)(2,1)}, bf16[512,256]{1,0:T(8,128)(2,1)S(1)}, u32[]{:S(2)}, u32[]{:S(2)}) collective-permute-start(bf16[512,256]{1,0:T(8,128)(2,1)} %collective-permute-done.13), channel_id=1, source_target_pairs={{1,0},{2,1},{3,2},{4,3},{5,4},{6,5},{7,6},{8,7},{9,8},{10,9},{11,1... | collective-permute-start | bytes 786440 | tf_op jit(solution)/shard_map/ppermute | solution.py:32
  86.3 5.3 %copy-start.8 = (f32[1,512]{1,0:T(1,128)S(1)}, f32[1,512]{1,0:T(1,128)}, u32[]{:S(2)}) copy-start(f32[1,512]{1,0:T(1,128)} %param.19) | copy-start | bytes 6148
  91.9 4.4 %copy-start.2 = (bf16[512,16,256]{0,2,1:T(8,128)(2,1)S(1)}, bf16[512,16,256]{0,2,1:T(8,128)(2,1)}, u32[]{:S(2)}) copy-start(bf16[512,16,256]{0,2,1:T(8,128)(2,1)} %copy.37) | copy-start | bytes 12582916
  100.5 69.4 %copy-start.10 = (bf16[1,4]{1,0:T(2,128)(2,1)S(1)}, bf16[1,4]{1,0:T(2,128)(2,1)}, u32[]{:S(2)}) copy-start(bf16[1,4]{1,0:T(2,128)(2,1)} %param.20) | copy-start | bytes 28
  100.5 93.7 %copy-start.9 = (bf16[128]{0:T(256)(128)(2,1)S(1)}, bf16[128]{0:T(256)(128)(2,1)}, u32[]{:S(2)}) copy-start(bf16[128]{0:T(256)(128)(2,1)} %param.21) | copy-start | bytes 772
  163.8 16.0 %all-to-all-start = ((f32[32,1,4,128]{3,2,1,0:T(4,128)}), f32[32,1,4,128]{3,2,1,0:T(4,128)S(1)}, u32[]{:S(2)}, u32[]{:S(2)}) async-start(f32[32,1,4,128]{3,2,1,0:T(4,128)} %copy.42), calls=%async_computation | async-start | bytes 131072 | tf_op jit(solution)/shard_map/all_to_all | solution.py:71
  179.8 14.8 %copy-start.7 = (bf16[4,128]{1,0:T(4,128)(2,1)}, bf16[4,128]{1,0:T(4,128)(2,1)S(1)}, u32[]{:S(2)}) copy-start(bf16[4,128]{1,0:T(4,128)(2,1)S(1)} %reduce_sum.46) | copy-start | bytes 3076
  (3 other events, 5.9 us)
